TPU v7x, 512 devices: a whole 4x8x8 slice. The times are simulated.
512 devices in a mesh: sp: 64 (over z, y), tp: 4 (over x), dp: 2 (over core).
Axes of the slice: x: 4, y: 8, z: 8, core: 2. Of those that a mesh axis runs over, the one named last changes fastest.
Arguments:
- latent: bfloat16 [2, 16384, 2048], P('dp', 'sp'), may hold values from -1.5 to 1.5
- condition: bfloat16 [2, 2048], P('dp', 'sp'), may hold values from -6 to 6
- context: bfloat16 [2, 1024, 2048], P('dp', 'sp'), may hold values from -6 to 6
- context_code: bfloat16 [2048], P('sp'), may hold values from -6 to 6
- shift_weight: bfloat16 [2048, 2048], P('sp', 'tp'), may hold values from -0.125 to 0.125
- scale_weight: bfloat16 [2048, 2048], P('sp', 'tp'), may hold values from -0.125 to 0.125
- gate_weight: bfloat16 [2048, 2048], P('sp', 'tp'), may hold values from -0.125 to 0.125
- norm_gain: float32 [2048], replicated, may hold values from 0.1 to 1.9
- query_weight: bfloat16 [2048, 1024], P(None, 'tp'), may hold values from -0.125 to 0.125
- key_weight: bfloat16 [2048, 256], P(None, 'tp'), may hold values from -0.125 to 0.125
- value_weight: bfloat16 [2048, 256], P(None, 'tp'), may hold values from -0.125 to 0.125
- output_weight: bfloat16 [1024, 2048], P('tp'), may hold values from -0.75 to 0.75
- query_gain: float32 [64], replicated, may hold values from 1 to 5.5
- key_gain: float32 [64], replicated, may hold values from 1 to 5.5
- context_bias: float32 [16], P('tp'), may hold values from 0.5 to 2
Outputs:
- updated: bfloat16 [2, 16384, 2048], P('dp', 'sp')
All inputs are finite; a program needn't handle non-finite values.
Results may differ from a plain program's by a relative error of at most 0.01405.
The roundings to bfloat16 on the way count: a program that leaves them out, or rounds other values in their place, can miss the bound.
Values may be sent and summed in bfloat16 or wider, within the bound.
A program may use at most 64 MiB of HBM per device.

v0:
```python
import math
import jax
import jax.numpy as jnp
from jax import lax
from jax.sharding import PartitionSpec as P

GRID_W = 64
norm_eps = 1e-06
rope_base = 10000.0


def from_everyone(array, axis):
    size = lax.axis_size(axis)
    return lax.all_to_all(
        jnp.broadcast_to(array[None], (size, *array.shape)), axis, 0, 0, tiled=True
    )


def of_everyone(array, axis):
    return from_everyone(array, axis).sum(axis=0)


def laid_out(pieces, dim):
    dims = list(pieces.shape[1:])
    dims[dim] *= pieces.shape[0]
    return jnp.moveaxis(pieces, 0, dim).reshape(dims)


def gathered_copies(array, axis, dim):
    pieces = from_everyone(array, axis)
    return laid_out(pieces, dim)


def cut_along(array, dim, size):
    before, after = (array.shape[:dim], array.shape[dim + 1 :])
    return jnp.moveaxis(array.reshape(*before, size, -1, *after), dim, 0)


def sent_and_summed(array, axis, dim):
    size = lax.axis_size(axis)
    pieces = lax.all_to_all(cut_along(array, dim, size), axis, 0, 0, tiled=True)
    return jnp.sum(pieces.astype(jnp.float32), axis=0)


def rotary_tables(position, grid_width, head_dim):
    grid_row = (position // grid_width).astype(jnp.float32)
    grid_col = (position % grid_width).astype(jnp.float32)
    quarter = head_dim // 4
    inverse = rope_base ** (-jnp.arange(quarter, dtype=jnp.float32) / quarter)
    angles = jnp.concatenate([grid_row[:, None] * inverse, grid_col[:, None] * inverse], axis=-1)
    return (jnp.cos(angles), jnp.sin(angles))


def head_norm(values, gain_row):
    return (
        values * lax.rsqrt(jnp.mean(values * values, axis=-1, keepdims=True) + norm_eps) * gain_row
    )


def rotate(values, cosine, sine_part):
    half_dim = values.shape[-1] // 2
    first_half = values[..., :half_dim]
    second_half = values[..., half_dim:]
    cos_rows = cosine[:, None, :]
    sin_rows = sine_part[:, None, :]
    return jnp.concatenate(
        [
            first_half * cos_rows - second_half * sin_rows,
            second_half * cos_rows + first_half * sin_rows,
        ],
        axis=-1,
    )


def modulated(tokens, gain_row, shift_row, scale_row):
    floats = tokens.astype(jnp.float32)
    normal = floats * lax.rsqrt(jnp.mean(floats * floats, axis=-1, keepdims=True) + norm_eps)
    return (normal * gain_row * (1.0 + scale_row) + shift_row).astype(jnp.bfloat16)


def on_device(
    latent,
    condition,
    context,
    context_code,
    shift_weight,
    scale_weight,
    gate_weight,
    norm_gain,
    query_weight,
    key_weight,
    value_weight,
    output_weight,
    query_gain,
    key_gain,
    context_bias,
):
    head_dim = query_gain.shape[0]
    tp_size = lax.axis_size("tp")
    activated = jax.nn.silu(condition[0].astype(jnp.float32)).astype(jnp.bfloat16)
    context_act = jax.nn.silu(context_code.astype(jnp.float32)).astype(jnp.bfloat16)
    partial_mod = jnp.stack(
        [
            jnp.dot(activated, shift_weight, preferred_element_type=jnp.float32),
            jnp.dot(activated, scale_weight, preferred_element_type=jnp.float32),
            jnp.dot(activated, gate_weight, preferred_element_type=jnp.float32),
            jnp.dot(context_act, shift_weight, preferred_element_type=jnp.float32),
            jnp.dot(context_act, scale_weight, preferred_element_type=jnp.float32),
        ]
    )
    summed = of_everyone(partial_mod, "sp")
    vectors = gathered_copies(summed, "tp", 1)
    normed = modulated(latent[0], norm_gain, vectors[0], vectors[1])
    query_cols = query_weight.shape[1]
    key_cols = key_weight.shape[1]
    projected = jnp.concatenate(
        [
            jnp.dot(normed, query_weight, preferred_element_type=jnp.float32),
            jnp.dot(normed, key_weight, preferred_element_type=jnp.float32),
            jnp.dot(normed, value_weight, preferred_element_type=jnp.float32),
        ],
        axis=1,
    )
    seq_rows = projected.shape[0]
    position = lax.axis_index("sp") * seq_rows + jnp.arange(seq_rows, dtype=jnp.int32)
    cosine, sine_part = rotary_tables(position, GRID_W, head_dim)
    group_size = query_cols // head_dim
    queries = projected[:, :query_cols].reshape(seq_rows, group_size, head_dim)
    queries = rotate(head_norm(queries, query_gain), cosine, sine_part).astype(jnp.bfloat16)
    latent_keys = projected[:, query_cols : query_cols + key_cols].reshape(seq_rows, 1, head_dim)
    latent_keys = rotate(head_norm(latent_keys, key_gain), cosine, sine_part).astype(jnp.bfloat16)
    latent_values = projected[:, query_cols + key_cols :].astype(jnp.bfloat16)
    key_value = jnp.concatenate([latent_keys.reshape(seq_rows, head_dim), latent_values], axis=1)
    context_normed = modulated(context[0], norm_gain, vectors[3], vectors[4])
    context_keys = head_norm(
        jnp.dot(context_normed, key_weight, preferred_element_type=jnp.float32), key_gain
    )
    context_values = jnp.dot(context_normed, value_weight, preferred_element_type=jnp.float32)
    context_kv = gathered_copies(
        jnp.concatenate(
            [context_keys.astype(jnp.bfloat16), context_values.astype(jnp.bfloat16)], axis=1
        ),
        "sp",
        0,
    )
    score_scale = head_dim ** (-0.5)
    query_rows = queries.transpose(1, 0, 2).reshape(group_size * seq_rows, head_dim)
    bias_rows = jnp.repeat(context_bias, seq_rows)
    context_scores = jnp.dot(
        query_rows, context_kv[:, :head_dim].T, preferred_element_type=jnp.float32
    )
    context_scores = context_scores * score_scale + bias_rows[:, None]
    first_max = context_scores.max(axis=1)
    context_exp = jnp.exp(context_scores - first_max[:, None])
    start_state = (
        first_max,
        context_exp.sum(axis=1),
        jnp.dot(
            context_exp.astype(jnp.bfloat16),
            context_kv[:, head_dim:],
            preferred_element_type=jnp.float32,
        ),
    )
    arrived = lax.all_gather(key_value, "sp", axis=0, tiled=True)
    arrived_rows = arrived.shape[0]
    block_rows = math.gcd(arrived_rows, 1024)
    blocks = arrived.reshape(arrived_rows // block_rows, block_rows, 2 * head_dim)

    def absorb_block(state_now, pair_block):
        old_max, old_total, old_accum = state_now
        scores = (
            jnp.dot(query_rows, pair_block[:, :head_dim].T, preferred_element_type=jnp.float32)
            * score_scale
        )
        new_max = jnp.maximum(old_max, scores.max(axis=1))
        factor = jnp.exp(old_max - new_max)
        weights = jnp.exp(scores - new_max[:, None])
        new_accum = old_accum * factor[:, None] + jnp.dot(
            weights.astype(jnp.bfloat16),
            pair_block[:, head_dim:],
            preferred_element_type=jnp.float32,
        )
        return ((new_max, old_total * factor + weights.sum(axis=1), new_accum), None)

    final_state, unused = lax.scan(absorb_block, start_state, blocks)
    row_max, totals, accum = final_state
    attended = (accum / totals[:, None]).astype(jnp.bfloat16)
    attended = (
        attended.reshape(group_size, seq_rows, head_dim)
        .transpose(1, 0, 2)
        .reshape(seq_rows, query_cols)
    )
    own_rows = seq_rows // tp_size
    mixed = sent_and_summed(
        jnp.dot(attended, output_weight, preferred_element_type=jnp.float32).astype(jnp.bfloat16),
        "tp",
        0,
    )
    own_latent = lax.dynamic_slice_in_dim(latent[0], lax.axis_index("tp") * own_rows, own_rows, 0)
    updated = (own_latent.astype(jnp.float32) + vectors[2] * mixed).astype(jnp.bfloat16)
    whole = gathered_copies(updated, "tp", 0)
    return whole[None]


def solution(mesh):
    return jax.shard_map(
        on_device,
        mesh=mesh,
        in_specs=(
            P("dp", "sp", None),
            P("dp", "sp"),
            P("dp", "sp", None),
            P("sp"),
            P("sp", "tp"),
            P("sp", "tp"),
            P("sp", "tp"),
            P(),
            P(None, "tp"),
            P(None, "tp"),
            P(None, "tp"),
            P("tp", None),
            P(),
            P(),
            P("tp"),
        ),
        out_specs=P("dp", "sp", None),
        check_vma=False,
    )
```

profile of v0, /device:TPU:8, one launch (start us, length us, event | category | flops | bytes accessed | tf_op | source)
XLA Modules:
  0.0 259.9 jit_solution(298645395595733858)
XLA Ops:
  6.5 1.0 fusion.59
  7.6 0.9 fusion.61
  8.5 0.9 fusion.67
  9.4 0.9 fusion.65
  10.3 0.9 fusion.63
  11.3 1.1 broadcast_in_dim.12
  12.4 16.6 %all-to-all-start = ((f32[64,5,512]{2,1,0:T(8,128)}), f32[64,5,512]{2,1,0:T(8,128)S(1)}, u32[]{:S(2)}, u32[]{:S(2)}) async-start(f32[64,5,512]{2,1,0:T(8,128)} %broadcast_in_dim.12), calls=%async_computation | async-start | bytes 2097152 | tf_op jit(solution)/shard_map/all_to_all | solution.py:14
  29.0 2.1 fusion.16
  31.2 27.1 %all-to-all-done = f32[64,5,512]{2,1,0:T(8,128)S(1)} async-done(((f32[64,5,512]{2,1,0:T(8,128)}), f32[64,5,512]{2,1,0:T(8,128)S(1)}, u32[]{:S(2)}, u32[]{:S(2)}) %all-to-all-start) | async-done | bytes 655392 | tf_op jit(solution)/shard_map/all_to_all | solution.py:14
  59.0 4.3 %all-to-all-start.1 = ((f32[4,5,512]{2,1,0:T(8,128)}), f32[4,5,512]{2,1,0:T(8,128)S(1)}, u32[]{:S(2)}, u32[]{:S(2)}) async-start(f32[4,5,512]{2,1,0:T(8,128)} %broadcast_in_dim.13), calls=%async_computation.1 | async-start | bytes 131072 | tf_op jit(solution)/shard_map/all_to_all | solution.py:14
  63.3 1.3 add_rsqrt_fusion.2
  64.6 4.3 %all-to-all-done.1 = f32[4,5,512]{2,1,0:T(8,128)S(1)} async-done(((f32[4,5,512]{2,1,0:T(8,128)}), f32[4,5,512]{2,1,0:T(8,128)S(1)}, u32[]{:S(2)}, u32[]{:S(2)}) %all-to-all-start.1) | async-done | bytes 40992 | tf_op jit(solution)/shard_map/all_to_all | solution.py:14
  69.5 1.6 convolution_convert_fusion.1
  71.2 1.3 multiply_reduce_fusion.2
  74.8 1.4 copy.33
  76.5 1.1 multiply_reduce_fusion.3
  77.6 0.7 multiply_convert_fusion
  78.3 1.2 convolution_convert_fusion.2
  79.6 0.7 broadcast_in_dim.14
  80.3 7.0 %all-to-all-start.2 = ((bf16[64,16,128]{2,1,0:T(8,128)(2,1)}), bf16[64,16,128]{2,1,0:T(8,128)(2,1)S(1)}, u32[]{:S(2)}, u32[]{:S(2)}) async-start(bf16[64,16,128]{2,1,0:T(8,128)(2,1)} %broadcast_in_dim.14), calls=%async_computation.2 | async-start | bytes 524288 | tf_op jit(solution)/shard_map/all_to_all | solution.py:14
  87.3 2.0 multiply_reduce_fusion.1
  89.7 10.9 %all-to-all-done.2 = bf16[64,16,128]{2,1,0:T(8,128)(2,1)S(1)} async-done(((bf16[64,16,128]{2,1,0:T(8,128)(2,1)}), bf16[64,16,128]{2,1,0:T(8,128)(2,1)S(1)}, u32[]{:S(2)}, u32[]{:S(2)}) %all-to-all-start.2) | async-done | bytes 262176 | tf_op jit(solution)/shard_map/all_to_all | solution.py:14
  101.2 0.9 fusion.13
  102.1 1.0 fusion.25
  103.1 57.5 %all-gather.2.cloned.1.call-done = bf16[16384,128]{0,1:T(8,128)(2,1)} async-done(((bf16[256,128]{0,1:T(8,128)(2,1)}), bf16[16384,128]{0,1:T(8,128)(2,1)}) %all-gather.2.cloned.1.call-update) | async-done | bytes 4194320 | tf_op jit(solution)/shard_map/all_gather | solution.py:164
  160.6 6.4 %copy.38 = bf16[16384,128]{1,0:T(8,128)(2,1)} copy(bf16[16384,128]{0,1:T(8,128)(2,1)} %all-gather.2.cloned.1.call-done) | data formatting | bytes 8388608 | tf_op jit(solution)/shard_map/while | solution.py:185
  167.0 54.7 %while.14 = (s32[]{:T(128)}, f32[1024]{0:T(1024)S(1)}, f32[1024]{0:T(1024)S(1)}, f32[1024,64]{0,1:T(8,128)S(1)}, bf16[16,1024,128]{2,1,0:T(8,128)(2,1)}, /*index=5*/bf16[1024,64]{1,0:T(8,128)(2,1)S(1)}, s32[]{:T(128)}) while((s32[]{:T(128)}, f32[1024]{0:T(1024)S(1)}, f32[1024]{0:T(1024)S(1)}, f32[1024,64]{0,1:T(8,128)S(1)}, ...), condition=%wide.region_11.12_spmd, body=%wide.region_8.11_spmd.sunk | while | flops 276957184 | bytes 14352473 | solution.py:185
  167.0 1.0 dynamic-slice_bitcast_fusion.2
  169.5 0.9 fusion.105
  170.4 1.0 dynamic-slice_bitcast_fusion.2
  172.9 0.9 fusion.105
  173.8 1.0 dynamic-slice_bitcast_fusion.2
  176.3 0.9 fusion.105
  177.2 1.0 dynamic-slice_bitcast_fusion.2
  179.7 0.9 fusion.105
  180.7 1.0 dynamic-slice_bitcast_fusion.2
  183.1 0.9 fusion.105
  184.1 1.0 dynamic-slice_bitcast_fusion.2
  186.5 0.9 fusion.105
  187.5 1.0 dynamic-slice_bitcast_fusion.2
  190.0 0.9 fusion.105
  190.9 1.0 dynamic-slice_bitcast_fusion.2
  193.4 0.9 fusion.105
  194.3 1.0 dynamic-slice_bitcast_fusion.2
  196.8 0.9 fusion.105
  197.8 1.0 dynamic-slice_bitcast_fusion.2
  200.2 0.9 fusion.105
  201.2 1.0 dynamic-slice_bitcast_fusion.2
  203.6 0.9 fusion.105
  204.6 1.0 dynamic-slice_bitcast_fusion.2
  207.1 0.9 fusion.105
  208.0 1.0 dynamic-slice_bitcast_fusion.2
  210.5 0.9 fusion.105
  211.4 1.0 dynamic-slice_bitcast_fusion.2
  213.9 0.9 fusion.105
  214.9 1.0 dynamic-slice_bitcast_fusion.2
  217.3 0.9 fusion.105
  218.3 1.0 dynamic-slice_bitcast_fusion.2
  220.7 0.9 fusion.105
  221.9 1.4 convolution_convert_fusion
  223.3 4.2 %all-to-all-start.3 = ((bf16[4,64,2048]{2,1,0:T(8,128)(2,1)}), bf16[4,64,2048]{2,1,0:T(8,128)(2,1)S(1)}, u32[]{:S(2)}, u32[]{:S(2)}) async-start(bf16[4,64,2048]{2,1,0:T(8,128)(2,1)} %bitcast.36), calls=%async_computation.3 | async-start | bytes 2097152 | tf_op jit(solution)/shard_map/all_to_all | solution.py:41
  227.5 10.9 %all-to-all-done.3 = bf16[4,64,2048]{2,1,0:T(8,128)(2,1)S(1)} async-done(((bf16[4,64,2048]{2,1,0:T(8,128)(2,1)}), bf16[4,64,2048]{2,1,0:T(8,128)(2,1)S(1)}, u32[]{:S(2)}, u32[]{:S(2)}) %all-to-all-start.3) | async-done | bytes 1048608 | tf_op jit(solution)/shard_map/all_to_all | solution.py:41
  238.8 13.3 %all_to_all.25 = bf16[4,64,2048]{2,1,0:T(8,128)(2,1)S(1)} all-to-all(bf16[4,64,2048]{2,1,0:T(8,128)(2,1)S(1)} %broadcast_in_dim.17), channel_id=1, replica_groups=mesh['sp'=64,'tp'=4,'dp'=2] {'tp'}, dimensions={0} | all-to-all | bytes 2097152 | tf_op jit(solution)/shard_map/all_to_all | solution.py:14
  252.1 1.0 copy.55
  (131 shorter events, 29.1 us)
Async XLA Ops:
  6.5 215.3 %copy-start = (bf16[256,2048]{1,0:T(8,128)(2,1)S(1)}, bf16[256,2048]{1,0:T(8,128)(2,1)}, u32[]{:S(2)}) copy-start(bf16[256,2048]{1,0:T(8,128)(2,1)} %param.28) | copy-start | bytes 3145732
  6.5 63.0 %copy-start.1 = (bf16[1,256,2048]{2,1,0:T(8,128)(2,1)S(1)}, bf16[1,256,2048]{2,1,0:T(8,128)(2,1)}, u32[]{:S(2)}) copy-start(bf16[1,256,2048]{2,1,0:T(8,128)(2,1)} %param.17) | copy-start | bytes 3145732
  11.2 59.9 %copy-start.4 = (bf16[2048,64]{0,1:T(8,128)(2,1)S(1)}, bf16[2048,64]{0,1:T(8,128)(2,1)}, u32[]{:S(2)}) copy-start(bf16[2048,64]{0,1:T(8,128)(2,1)} %param.26) | copy-start | bytes 786436
  12.4 45.9 %all-to-all-start = ((f32[64,5,512]{2,1,0:T(8,128)}), f32[64,5,512]{2,1,0:T(8,128)S(1)}, u32[]{:S(2)}, u32[]{:S(2)}) async-start(f32[64,5,512]{2,1,0:T(8,128)} %broadcast_in_dim.12), calls=%async_computation | async-start | bytes 2097152 | tf_op jit(solution)/shard_map/all_to_all | solution.py:14
  58.3 16.5 %copy-start.2 = (bf16[2048,256]{1,0:T(8,128)(2,1)S(1)}, bf16[2048,256]{1,0:T(8,128)(2,1)}, u32[]{:S(2)}) copy-start(bf16[2048,256]{1,0:T(8,128)(2,1)} %param.25) | copy-start | bytes 3145732
  59.0 9.9 %all-to-all-start.1 = ((f32[4,5,512]{2,1,0:T(8,128)}), f32[4,5,512]{2,1,0:T(8,128)S(1)}, u32[]{:S(2)}, u32[]{:S(2)}) async-start(f32[4,5,512]{2,1,0:T(8,128)} %broadcast_in_dim.13), calls=%async_computation.1 | async-start | bytes 131072 | tf_op jit(solution)/shard_map/all_to_all | solution.py:14
  63.3 97.3 %all-gather.2.cloned.1.call-start = ((), (), s32[]{:S(2)}) async-start(), calls=%async_computation.5 | async-start | bytes 4259840 | tf_op jit(solution)/shard_map/all_gather | solution.py:164
  69.5 3.9 %copy-start.6 = (f32[1,4,512]{2,0,1:T(1,128)}, f32[1,4,512]{2,0,1:T(1,128)S(1)}, u32[]{:S(2)}) copy-start(f32[1,4,512]{2,0,1:T(1,128)S(1)} %get-tuple-element.93) | copy-start | bytes 24580
  69.5 3.9 %copy-start.7 = (f32[1,4,512]{2,0,1:T(1,128)}, f32[1,4,512]{2,0,1:T(1,128)S(1)}, u32[]{:S(2)}) copy-start(f32[1,4,512]{2,0,1:T(1,128)S(1)} %get-tuple-element.94) | copy-start | bytes 24580
  69.5 6.8 %copy-start.3 = (bf16[1,16,2048]{2,1,0:T(8,128)(2,1)S(1)}, bf16[1,16,2048]{2,1,0:T(8,128)(2,1)}, u32[]{:S(2)}) copy-start(bf16[1,16,2048]{2,1,0:T(8,128)(2,1)} %param.19) | copy-start | bytes 196612
  74.8 14.5 %copy-start.8 = (f32[64]{0:T(128)S(1)}, f32[64]{0:T(128)}, u32[]{:S(2)}) copy-start(f32[64]{0:T(128)} %param.29) | copy-start | bytes 772
  80.3 20.2 %all-to-all-start.2 = ((bf16[64,16,128]{2,1,0:T(8,128)(2,1)}), bf16[64,16,128]{2,1,0:T(8,128)(2,1)S(1)}, u32[]{:S(2)}, u32[]{:S(2)}) async-start(bf16[64,16,128]{2,1,0:T(8,128)(2,1)} %broadcast_in_dim.14), calls=%async_computation.2 | async-start | bytes 524288 | tf_op jit(solution)/shard_map/all_to_all | solution.py:14
  221.7 16.9 %copy-start.5 = (f32[1,4,512]{2,0,1:T(1,128)S(1)}, f32[1,4,512]{2,0,1:T(1,128)}, u32[]{:S(2)}) copy-start(f32[1,4,512]{2,0,1:T(1,128)} %get-tuple-element.90) | copy-start | bytes 24580
  223.3 15.1 %all-to-all-start.3 = ((bf16[4,64,2048]{2,1,0:T(8,128)(2,1)}), bf16[4,64,2048]{2,1,0:T(8,128)(2,1)S(1)}, u32[]{:S(2)}, u32[]{:S(2)}) async-start(bf16[4,64,2048]{2,1,0:T(8,128)(2,1)} %bitcast.36), calls=%async_computation.3 | async-start | bytes 2097152 | tf_op jit(solution)/shard_map/all_to_all | solution.py:41
Sparse Core Ops, SparseCore 0:
  74.2 86.3 all-gather.1
where the time goes:
time: 261 us; the launch traced here: 260 us
  waiting for transfers between devices  111 us (43%)
  matrix products  41.4 us (16%)
  starting transfers between devices  32.1 us (12%)
  local copies, waits for them, and re-layouts  28 us (11%)
  other arithmetic  20 us (8%)
  between operations  13.7 us (5%)
  blocking collectives  13.3 us (5%)
    all_gather x1, waiting for transfers between devices, on_device(): arrived = lax.all_gather(key_value, 'sp', axis=0, tiled=True)  57.5 us
    all_to_all x3, waiting for transfers between devices, from_everyone(): lax.all_to_all(jnp.broadcast_to(array[None], (size, *array.shape)), axis,...  42.3 us
    all_to_all x3, starting transfers between devices, from_everyone(): lax.all_to_all(jnp.broadcast_to(array[None], (size, *array.shape)), axis,...  27.8 us
    squeeze x16, local copies, waits for them, and re-layouts, on_device(): final_state, unused = lax.scan(absorb_block, start_state, blocks)  15.5 us
    dot_general x16, matrix products, absorb_block(): jnp.dot(weights.astype(jnp.bfloat16), pair_block[:, head_dim:], preferred...  14.9 us
    all_to_all x1, blocking collectives, from_everyone(): lax.all_to_all(jnp.broadcast_to(array[None], (size, *array.shape)), axis,...  13.3 us
    reduce_sum x16, other arithmetic, absorb_block(): weights.sum(axis=1)  11.7 us
    dot_general x16, matrix products, absorb_block(): jnp.dot(query_rows, pair_block[:, :head_dim].T, preferred_element_type=jn...  11.5 us
  transfers between devices with their start and end apart: 5, of which 5 were waited for; matrix products, arithmetic and copies ran while one was open for 6% of the time, Pallas kernels for 0%

commit v1 on v0

--- a/solution.py
+++ b/solution.py
@@ -161,7 +161,17 @@
             preferred_element_type=jnp.float32,
         ),
     )
-    arrived = lax.all_gather(key_value, "sp", axis=0, tiled=True)
+    u_next, spare = (lax.axis_size("sp"), lax.axis_index("sp"))
+    arrived, f_next = (key_value, 1)
+    while f_next < u_next:
+        row_list = []
+        for src_i in range(u_next):
+            row_list.append((src_i, src_i ^ f_next))
+        out_arr = lax.ppermute(arrived, axis_name="sp", perm=row_list)
+        low = jnp.concatenate([arrived, out_arr], 0)
+        e_now = jnp.concatenate([out_arr, arrived], 0)
+        arrived = jnp.where(spare & f_next == 0, low, e_now)
+        f_next = 2 * f_next
     arrived_rows = arrived.shape[0]
     block_rows = math.gcd(arrived_rows, 1024)
     blocks = arrived.reshape(arrived_rows // block_rows, block_rows, 2 * head_dim)

time: 261 us -> 362 us (1.39)
  the two profiles are of different devices: /device:TPU:8 before, /device:TPU:192 now
where the time goes in v1:
time: 362 us; the launch traced here: 360 us
  waiting for transfers between devices  189 us (52%)
  starting transfers between devices  53.5 us (15%)
  matrix products  40.1 us (11%)
  local copies, waits for them, and re-layouts  30.1 us (8%)
  other arithmetic  29.2 us (8%)
  blocking collectives  16.8 us (5%)
    ppermute x6, waiting for transfers between devices, on_device(): out_arr = lax.ppermute(arrived, axis_name='sp', perm=row_list)  141 us
    all_to_all x3, waiting for transfers between devices, from_everyone(): lax.all_to_all(jnp.broadcast_to(array[None], (size, *array.shape)), axis,...  32.6 us
    all_to_all x3, starting transfers between devices, from_everyone(): lax.all_to_all(jnp.broadcast_to(array[None], (size, *array.shape)), axis,...  29.5 us
    ppermute x6, starting transfers between devices, on_device(): out_arr = lax.ppermute(arrived, axis_name='sp', perm=row_list)  20.5 us
    all_to_all x1, blocking collectives, from_everyone(): lax.all_to_all(jnp.broadcast_to(array[None], (size, *array.shape)), axis,...  16.8 us
    squeeze x16, local copies, waits for them, and re-layouts, on_device(): final_state, unused = lax.scan(absorb_block, start_state, blocks)  15.5 us
    all_to_all x1, waiting for transfers between devices, sent_and_summed(): pieces = lax.all_to_all(cut_along(array, dim, size), axis, 0, 0, tiled=True)  15.2 us
    dot_general x16, matrix products, absorb_block(): jnp.dot(weights.astype(jnp.bfloat16), pair_block[:, head_dim:], preferred...  14.9 us
  transfers between devices with their start and end apart: 10, of which 9 were waited for; matrix products, arithmetic and copies ran while one was open for 5% of the time, Pallas kernels for 0%

profile of v1, /device:TPU:192, one launch (start us, length us, event | category | flops | bytes accessed | tf_op | source)
XLA Modules:
  0.0 359.7 jit_solution(6491564052675328995)
XLA Ops:
  0.0 1.0 fusion.59
  4.7 1.1 broadcast_in_dim.12
  5.8 14.0 %all-to-all-start = ((f32[64,5,512]{2,1,0:T(8,128)}), f32[64,5,512]{2,1,0:T(8,128)S(1)}, u32[]{:S(2)}, u32[]{:S(2)}) async-start(f32[64,5,512]{2,1,0:T(8,128)} %broadcast_in_dim.12), calls=%async_computation | async-start | bytes 2097152 | tf_op jit(solution)/shard_map/all_to_all | solution.py:14
  19.9 1.5 fusion.16
  22.1 27.0 %all-to-all-done = f32[64,5,512]{2,1,0:T(8,128)S(1)} async-done(((f32[64,5,512]{2,1,0:T(8,128)}), f32[64,5,512]{2,1,0:T(8,128)S(1)}, u32[]{:S(2)}, u32[]{:S(2)}) %all-to-all-start) | async-done | bytes 655392 | tf_op jit(solution)/shard_map/all_to_all | solution.py:14
  49.8 4.3 %all-to-all-start.1 = ((f32[4,5,512]{2,1,0:T(8,128)}), f32[4,5,512]{2,1,0:T(8,128)S(1)}, u32[]{:S(2)}, u32[]{:S(2)}) async-start(f32[4,5,512]{2,1,0:T(8,128)} %broadcast_in_dim.13), calls=%async_computation.1 | async-start | bytes 131072 | tf_op jit(solution)/shard_map/all_to_all | solution.py:14
  54.1 5.6 %all-to-all-done.1 = f32[4,5,512]{2,1,0:T(8,128)S(1)} async-done(((f32[4,5,512]{2,1,0:T(8,128)}), f32[4,5,512]{2,1,0:T(8,128)S(1)}, u32[]{:S(2)}, u32[]{:S(2)}) %all-to-all-start.1) | async-done | bytes 40992 | tf_op jit(solution)/shard_map/all_to_all | solution.py:14
  60.4 1.6 convolution_convert_fusion.1
  62.0 1.3 multiply_reduce_fusion.2
  64.3 3.4 collective-permute-start
  67.7 2.7 collective-permute-done
  70.5 1.9 collective-permute-start.1
  72.4 7.3 %collective-permute-done.1 = bf16[512,128]{0,1:T(8,128)(2,1)S(1)} collective-permute-done((bf16[512,128]{0,1:T(8,128)(2,1)S(1)}, bf16[512,128]{0,1:T(8,128)(2,1)S(1)}, u32[]{:S(2)}, u32[]{:S(2)}) %collective-permute-start.1) | collective-permute-done | bytes 131104 | tf_op jit(solution)/shard_map/ppermute | solution.py:170
  79.8 3.7 %collective-permute-start.2 = (bf16[1024,128]{0,1:T(8,128)(2,1)S(1)}, bf16[1024,128]{0,1:T(8,128)(2,1)S(1)}, u32[]{:S(2)}, u32[]{:S(2)}) collective-permute-start(bf16[1024,128]{0,1:T(8,128)(2,1)S(1)} %maximum_select_fusion.4), channel_id=1, source_target_pairs={{0,32},{8,40},{16,48},{24,56},{32,0},{40,8},{48,16},{56,24},{64,96... | collective-permute-start | bytes 786440 | tf_op jit(solution)/shard_map/ppermute | solution.py:170
  83.5 8.9 %collective-permute-done.2 = bf16[1024,128]{0,1:T(8,128)(2,1)S(1)} collective-permute-done((bf16[1024,128]{0,1:T(8,128)(2,1)S(1)}, bf16[1024,128]{0,1:T(8,128)(2,1)S(1)}, u32[]{:S(2)}, u32[]{:S(2)}) %collective-permute-start.2) | collective-permute-done | bytes 262176 | tf_op jit(solution)/shard_map/ppermute | solution.py:170
  92.6 5.6 %collective-permute-start.3 = (bf16[2048,128]{0,1:T(8,128)(2,1)S(1)}, bf16[2048,128]{0,1:T(8,128)(2,1)S(1)}, u32[]{:S(2)}, u32[]{:S(2)}) collective-permute-start(bf16[2048,128]{0,1:T(8,128)(2,1)S(1)} %maximum_select_fusion.3), channel_id=1, source_target_pairs={{0,64},{8,72},{16,80},{24,88},{32,96},{40,104},{48,112},{56,120},{... | collective-permute-start | bytes 1572872 | tf_op jit(solution)/shard_map/ppermute | solution.py:170
  99.6 9.1 %collective-permute-done.3 = bf16[2048,128]{0,1:T(8,128)(2,1)S(1)} collective-permute-done((bf16[2048,128]{0,1:T(8,128)(2,1)S(1)}, bf16[2048,128]{0,1:T(8,128)(2,1)S(1)}, u32[]{:S(2)}, u32[]{:S(2)}) %collective-permute-start.3) | collective-permute-done | bytes 524320 | tf_op jit(solution)/shard_map/ppermute | solution.py:170
  108.9 1.9 collective-permute-start.4
  111.8 1.3 copy.41
  113.0 2.3 copy.33
  115.3 1.0 multiply_reduce_fusion.3
  117.1 1.2 convolution_convert_fusion.2
  119.2 11.2 %all-to-all-start.2 = ((bf16[64,16,128]{2,1,0:T(8,128)(2,1)}), bf16[64,16,128]{2,1,0:T(8,128)(2,1)S(1)}, u32[]{:S(2)}, u32[]{:S(2)}) async-start(bf16[64,16,128]{2,1,0:T(8,128)(2,1)} %broadcast_in_dim.14), calls=%async_computation.2 | async-start | bytes 524288 | tf_op jit(solution)/shard_map/all_to_all | solution.py:14
  130.4 24.1 %collective-permute-done.4 = bf16[4096,128]{0,1:T(8,128)(2,1)} collective-permute-done((bf16[4096,128]{0,1:T(8,128)(2,1)S(1)}, bf16[4096,128]{0,1:T(8,128)(2,1)}, u32[]{:S(2)}, u32[]{:S(2)}) %collective-permute-start.4) | collective-permute-done | bytes 1048608 | tf_op jit(solution)/shard_map/ppermute | solution.py:170
  154.5 3.3 maximum_select_fusion.1
  157.9 3.9 %collective-permute-start.5 = (bf16[8192,128]{0,1:T(8,128)(2,1)}, bf16[8192,128]{0,1:T(8,128)(2,1)}, u32[]{:S(2)}, u32[]{:S(2)}) collective-permute-start(bf16[8192,128]{0,1:T(8,128)(2,1)} %maximum_select_fusion.1), channel_id=1, source_target_pairs={{0,256},{8,264},{16,272},{24,280},{32,288},{40,296},{48,304},{56,3... | collective-permute-start | bytes 6291464 | tf_op jit(solution)/shard_map/ppermute | solution.py:170
  164.5 1.0 fusion.25
  165.6 88.5 %collective-permute-done.5 = bf16[8192,128]{0,1:T(8,128)(2,1)} collective-permute-done((bf16[8192,128]{0,1:T(8,128)(2,1)}, bf16[8192,128]{0,1:T(8,128)(2,1)}, u32[]{:S(2)}, u32[]{:S(2)}) %collective-permute-start.5) | collective-permute-done | bytes 2097184 | tf_op jit(solution)/shard_map/ppermute | solution.py:170
  254.1 6.0 %maximum_select_fusion = bf16[16384,128]{0,1:T(8,128)(2,1)} fusion(bf16[8192,128]{0,1:T(8,128)(2,1)} %collective-permute-done.5, bf16[8192,128]{0,1:T(8,128)(2,1)} %maximum_select_fusion.1, pred[]{:T(512)S(6)} %eq.20), kind=kLoop, calls=%fused_computation.13 | loop fusion | flops 18874368 | bytes 8388609 | tf_op jit(solution)/shard_map/jit(_where)/select_n | solution.py:173
  260.1 6.4 %copy.38 = bf16[16384,128]{1,0:T(8,128)(2,1)} copy(bf16[16384,128]{0,1:T(8,128)(2,1)} %maximum_select_fusion) | data formatting | bytes 8388608 | tf_op jit(solution)/shard_map/while | solution.py:195
  266.4 54.7 %while.14 = (s32[]{:T(128)}, f32[1024]{0:T(1024)S(1)}, f32[1024]{0:T(1024)S(1)}, f32[1024,64]{0,1:T(8,128)S(1)}, bf16[16,1024,128]{2,1,0:T(8,128)(2,1)}, /*index=5*/bf16[1024,64]{1,0:T(8,128)(2,1)S(1)}, s32[]{:T(128)}) while((s32[]{:T(128)}, f32[1024]{0:T(1024)S(1)}, f32[1024]{0:T(1024)S(1)}, f32[1024,64]{0,1:T(8,128)S(1)}, ...), condition=%wide.region_11.12_spmd, body=%wide.region_8.11_spmd.sunk | while | flops 276957184 | bytes 14352473 | solution.py:195
  266.4 1.0 dynamic-slice_bitcast_fusion.2
  268.9 0.9 fusion.105
  269.8 1.0 dynamic-slice_bitcast_fusion.2
  272.3 0.9 fusion.105
  273.3 1.0 dynamic-slice_bitcast_fusion.2
  275.7 0.9 fusion.105
  276.7 1.0 dynamic-slice_bitcast_fusion.2
  279.1 0.9 fusion.105
  280.1 1.0 dynamic-slice_bitcast_fusion.2
  282.6 0.9 fusion.105
  283.5 1.0 dynamic-slice_bitcast_fusion.2
  286.0 0.9 fusion.105
  286.9 1.0 dynamic-slice_bitcast_fusion.2
  289.4 0.9 fusion.105
  290.4 1.0 dynamic-slice_bitcast_fusion.2
  292.8 0.9 fusion.105
  293.8 1.0 dynamic-slice_bitcast_fusion.2
  296.2 0.9 fusion.105
  297.2 1.0 dynamic-slice_bitcast_fusion.2
  299.7 0.9 fusion.105
  300.6 1.0 dynamic-slice_bitcast_fusion.2
  303.1 0.9 fusion.105
  304.0 1.0 dynamic-slice_bitcast_fusion.2
  306.5 0.9 fusion.105
  307.5 1.0 dynamic-slice_bitcast_fusion.2
  310.9 1.0 dynamic-slice_bitcast_fusion.2
  314.3 1.0 dynamic-slice_bitcast_fusion.2
  317.7 1.0 dynamic-slice_bitcast_fusion.2
  321.3 1.4 convolution_convert_fusion
  322.7 3.5 all-to-all-start.3
  326.2 15.2 %all-to-all-done.3 = bf16[4,64,2048]{2,1,0:T(8,128)(2,1)S(1)} async-done(((bf16[4,64,2048]{2,1,0:T(8,128)(2,1)}), bf16[4,64,2048]{2,1,0:T(8,128)(2,1)S(1)}, u32[]{:S(2)}, u32[]{:S(2)}) %all-to-all-start.3) | async-done | bytes 1048608 | tf_op jit(solution)/shard_map/all_to_all | solution.py:41
  341.8 16.8 %all_to_all.25 = bf16[4,64,2048]{2,1,0:T(8,128)(2,1)S(1)} all-to-all(bf16[4,64,2048]{2,1,0:T(8,128)(2,1)S(1)} %broadcast_in_dim.17), channel_id=1, replica_groups=mesh['sp'=64,'tp'=4,'dp'=2] {'tp'}, dimensions={0} | all-to-all | bytes 2097152 | tf_op jit(solution)/shard_map/all_to_all | solution.py:14
  358.7 1.0 copy.55
  (166 shorter events, 41.2 us)
Async XLA Ops:
  0.0 321.3 %copy-start = (bf16[256,2048]{1,0:T(8,128)(2,1)S(1)}, bf16[256,2048]{1,0:T(8,128)(2,1)}, u32[]{:S(2)}) copy-start(bf16[256,2048]{1,0:T(8,128)(2,1)} %param.28) | copy-start | bytes 3145732
  0.0 60.4 %copy-start.1 = (bf16[1,256,2048]{2,1,0:T(8,128)(2,1)S(1)}, bf16[1,256,2048]{2,1,0:T(8,128)(2,1)}, u32[]{:S(2)}) copy-start(bf16[1,256,2048]{2,1,0:T(8,128)(2,1)} %param.17) | copy-start | bytes 3145732
  0.0 60.4 %copy-start.9 = (f32[2048]{0:T(1024)S(1)}, f32[2048]{0:T(1024)}, u32[]{:S(2)}) copy-start(f32[2048]{0:T(1024)} %param.24) | copy-start | bytes 24580
  4.7 57.3 %copy-start.4 = (bf16[2048,64]{0,1:T(8,128)(2,1)S(1)}, bf16[2048,64]{0,1:T(8,128)(2,1)}, u32[]{:S(2)}) copy-start(bf16[2048,64]{0,1:T(8,128)(2,1)} %param.26) | copy-start | bytes 786436
  5.8 43.2 %all-to-all-start = ((f32[64,5,512]{2,1,0:T(8,128)}), f32[64,5,512]{2,1,0:T(8,128)S(1)}, u32[]{:S(2)}, u32[]{:S(2)}) async-start(f32[64,5,512]{2,1,0:T(8,128)} %broadcast_in_dim.12), calls=%async_computation | async-start | bytes 2097152 | tf_op jit(solution)/shard_map/all_to_all | solution.py:14
  49.2 14.9 %copy-start.5 = (f32[256,1,16]{0,2,1:T(8,128)S(1)}, f32[256,1,16]{0,2,1:T(8,128)}, u32[]{:S(2)}) copy-start(f32[256,1,16]{0,2,1:T(8,128)} %get-tuple-element.97) | copy-start | bytes 49156
  49.2 14.9 %copy-start.6 = (f32[256,1,16]{0,2,1:T(8,128)S(1)}, f32[256,1,16]{0,2,1:T(8,128)}, u32[]{:S(2)}) copy-start(f32[256,1,16]{0,2,1:T(8,128)} %get-tuple-element.102) | copy-start | bytes 49156
  49.8 9.9 %all-to-all-start.1 = ((f32[4,5,512]{2,1,0:T(8,128)}), f32[4,5,512]{2,1,0:T(8,128)S(1)}, u32[]{:S(2)}, u32[]{:S(2)}) async-start(f32[4,5,512]{2,1,0:T(8,128)} %broadcast_in_dim.13), calls=%async_computation.1 | async-start | bytes 131072 | tf_op jit(solution)/shard_map/all_to_all | solution.py:14
  54.1 9.2 %copy-start.15 = (f32[256]{0:T(256)}, f32[256]{0:T(256)S(1)}, u32[]{:S(2)}) copy-start(f32[256]{0:T(256)S(1)} %add_rsqrt_fusion.2) | copy-start | bytes 3076
  60.4 3.9 %copy-start.11 = (f32[1,4,512]{2,0,1:T(1,128)}, f32[1,4,512]{2,0,1:T(1,128)S(1)}, u32[]{:S(2)}) copy-start(f32[1,4,512]{2,0,1:T(1,128)S(1)} %get-tuple-element.93) | copy-start | bytes 24580
  60.4 3.9 %copy-start.13 = (f32[1,4,512]{2,0,1:T(1,128)}, f32[1,4,512]{2,0,1:T(1,128)S(1)}, u32[]{:S(2)}) copy-start(f32[1,4,512]{2,0,1:T(1,128)S(1)} %get-tuple-element.94) | copy-start | bytes 24580
  60.4 37.8 %copy-start.3 = (bf16[1,16,2048]{2,1,0:T(8,128)(2,1)S(1)}, bf16[1,16,2048]{2,1,0:T(8,128)(2,1)}, u32[]{:S(2)}) copy-start(bf16[1,16,2048]{2,1,0:T(8,128)(2,1)} %param.19) | copy-start | bytes 196612
  60.4 38.5 %copy-start.18 = (f32[4]{0:T(128)S(1)}, f32[4]{0:T(128)}, u32[]{:S(2)}) copy-start(f32[4]{0:T(128)} %param.31) | copy-start | bytes 52
  64.3 6.2 %collective-permute-start = (bf16[256,128]{0,1:T(8,128)(2,1)S(1)}, bf16[256,128]{0,1:T(8,128)(2,1)S(1)}, u32[]{:S(2)}, u32[]{:S(2)}) collective-permute-start(bf16[256,128]{0,1:T(8,128)(2,1)S(1)} %pad_maximum_fusion), channel_id=1, source_target_pairs={{0,8},{8,0},{16,24},{24,16},{32,40},{40,32},{48,56},{56,48},{64,72... | collective-permute-start | bytes 196616 | tf_op jit(solution)/shard_map/ppermute | solution.py:170
  70.5 9.3 %collective-permute-start.1 = (bf16[512,128]{0,1:T(8,128)(2,1)S(1)}, bf16[512,128]{0,1:T(8,128)(2,1)S(1)}, u32[]{:S(2)}, u32[]{:S(2)}) collective-permute-start(bf16[512,128]{0,1:T(8,128)(2,1)S(1)} %maximum_select_fusion.5), channel_id=1, source_target_pairs={{0,16},{8,24},{16,0},{24,8},{32,48},{40,56},{48,32},{56,40},{64,80... | collective-permute-start | bytes 393224 | tf_op jit(solution)/shard_map/ppermute | solution.py:170
  79.8 12.6 %collective-permute-start.2 = (bf16[1024,128]{0,1:T(8,128)(2,1)S(1)}, bf16[1024,128]{0,1:T(8,128)(2,1)S(1)}, u32[]{:S(2)}, u32[]{:S(2)}) collective-permute-start(bf16[1024,128]{0,1:T(8,128)(2,1)S(1)} %maximum_select_fusion.4), channel_id=1, source_target_pairs={{0,32},{8,40},{16,48},{24,56},{32,0},{40,8},{48,16},{56,24},{64,96... | collective-permute-start | bytes 786440 | tf_op jit(solution)/shard_map/ppermute | solution.py:170
  92.6 16.1 %collective-permute-start.3 = (bf16[2048,128]{0,1:T(8,128)(2,1)S(1)}, bf16[2048,128]{0,1:T(8,128)(2,1)S(1)}, u32[]{:S(2)}, u32[]{:S(2)}) collective-permute-start(bf16[2048,128]{0,1:T(8,128)(2,1)S(1)} %maximum_select_fusion.3), channel_id=1, source_target_pairs={{0,64},{8,72},{16,80},{24,88},{32,96},{40,104},{48,112},{56,120},{... | collective-permute-start | bytes 1572872 | tf_op jit(solution)/shard_map/ppermute | solution.py:170
  108.9 45.6 %collective-permute-start.4 = (bf16[4096,128]{0,1:T(8,128)(2,1)S(1)}, bf16[4096,128]{0,1:T(8,128)(2,1)}, u32[]{:S(2)}, u32[]{:S(2)}) collective-permute-start(bf16[4096,128]{0,1:T(8,128)(2,1)S(1)} %maximum_select_fusion.2), channel_id=1, source_target_pairs={{0,128},{8,136},{16,144},{24,152},{32,160},{40,168},{48,176},{56,1... | collective-permute-start | bytes 3145736 | tf_op jit(solution)/shard_map/ppermute | solution.py:170
  116.3 45.5 %copy-start.10 = (f32[2048]{0:T(1024)S(1)}, f32[2048]{0:T(1024)}, u32[]{:S(2)}) copy-start(f32[2048]{0:T(1024)} %param.24) | copy-start | bytes 24580
  116.4 45.5 %copy-start.12 = (f32[1,4,512]{2,0,1:T(1,128)S(1)}, f32[1,4,512]{2,0,1:T(1,128)}, u32[]{:S(2)}) copy-start(f32[1,4,512]{2,0,1:T(1,128)} %copy-done.11) | copy-start | bytes 24580
  116.4 45.5 %copy-start.14 = (f32[1,4,512]{2,0,1:T(1,128)S(1)}, f32[1,4,512]{2,0,1:T(1,128)}, u32[]{:S(2)}) copy-start(f32[1,4,512]{2,0,1:T(1,128)} %copy-done.13) | copy-start | bytes 24580
  116.4 45.5 %copy-start.16 = (f32[256]{0:T(256)S(1)}, f32[256]{0:T(256)}, u32[]{:S(2)}) copy-start(f32[256]{0:T(256)} %copy-done.15) | copy-start | bytes 3076
  119.2 43.8 %all-to-all-start.2 = ((bf16[64,16,128]{2,1,0:T(8,128)(2,1)}), bf16[64,16,128]{2,1,0:T(8,128)(2,1)S(1)}, u32[]{:S(2)}, u32[]{:S(2)}) async-start(bf16[64,16,128]{2,1,0:T(8,128)(2,1)} %broadcast_in_dim.14), calls=%async_computation.2 | async-start | bytes 524288 | tf_op jit(solution)/shard_map/all_to_all | solution.py:14
  130.4 31.5 %copy-start.2 = (bf16[2048,256]{0,1:T(8,128)(2,1)S(1)}, bf16[2048,256]{0,1:T(8,128)(2,1)}, u32[]{:S(2)}) copy-start(bf16[2048,256]{0,1:T(8,128)(2,1)} %copy.33) | copy-start | bytes 3145732
  130.4 32.2 %copy-start.17 = (f32[64]{0:T(128)S(1)}, f32[64]{0:T(128)}, u32[]{:S(2)}) copy-start(f32[64]{0:T(128)} %param.29) | copy-start | bytes 772
  157.9 5.1 %copy-start.7 = (f32[1,2,4,128]{3,1,2,0:T(2,128)S(1)}, f32[1,2,4,128]{3,1,2,0:T(2,128)}, u32[]{:S(2)}) copy-start(f32[1,2,4,128]{3,1,2,0:T(2,128)} %copy.41) | copy-start | bytes 12292
  157.9 96.2 %collective-permute-start.5 = (bf16[8192,128]{0,1:T(8,128)(2,1)}, bf16[8192,128]{0,1:T(8,128)(2,1)}, u32[]{:S(2)}, u32[]{:S(2)}) collective-permute-start(bf16[8192,128]{0,1:T(8,128)(2,1)} %maximum_select_fusion.1), channel_id=1, source_target_pairs={{0,256},{8,264},{16,272},{24,280},{32,288},{40,296},{48,304},{56,3... | collective-permute-start | bytes 6291464 | tf_op jit(solution)/shard_map/ppermute | solution.py:170
  321.1 20.5 %copy-start.8 = (f32[1,4,512]{2,0,1:T(1,128)S(1)}, f32[1,4,512]{2,0,1:T(1,128)}, u32[]{:S(2)}) copy-start(f32[1,4,512]{2,0,1:T(1,128)} %get-tuple-element.90) | copy-start | bytes 24580
  322.7 18.8 %all-to-all-start.3 = ((bf16[4,64,2048]{2,1,0:T(8,128)(2,1)}), bf16[4,64,2048]{2,1,0:T(8,128)(2,1)S(1)}, u32[]{:S(2)}, u32[]{:S(2)}) async-start(bf16[4,64,2048]{2,1,0:T(8,128)(2,1)} %bitcast.36), calls=%async_computation.3 | async-start | bytes 2097152 | tf_op jit(solution)/shard_map/all_to_all | solution.py:41
